TPU v7x, 128 devices: a whole 4x4x4 slice. The times are simulated.
128 devices in a mesh: sp: 16 (over z, x), tp: 8 (over y, core).
Axes of the slice: x: 4, y: 4, z: 4, core: 2. Of those that a mesh axis runs over, the one named last changes fastest.
Arguments:
- tokens_in: bfloat16 [12288, 2048], P(('sp', 'tp')), may hold values from -300 to 300
- norm_gain: float32 [2048], replicated, may hold values from 0.1 to 1.9
- query_weight: bfloat16 [2048, 1024], P('sp', 'tp'), may hold values from -64 to 64
- key_weight: bfloat16 [2048, 512], P('sp', 'tp'), may hold values from -1 to 1
- value_weight: bfloat16 [2048, 512], P('sp', 'tp'), may hold values from -0.125 to 0.125
- pool_weight: bfloat16 [2048, 1024], P('sp', 'tp'), may hold values from -0.125 to 0.125
- sink_logit: float32 [16], P('tp'), may hold values from 1 to 5
- pool_gain: float32 [1024], P('tp'), may hold values from 0.1 to 1.9
- attention_out_weight: bfloat16 [1024, 2048], P('tp', 'sp'), may hold values from -0.125 to 0.125
- pool_out_weight: bfloat16 [1024, 2048], P('tp', 'sp'), may hold values from -0.1875 to 0.1875
Outputs:
- mixed_out: bfloat16 [12288, 2048], P(('sp', 'tp'))
All inputs are finite; a program needn't handle non-finite values.
Results may differ from a plain program's by a relative error of at most 0.014.
Values may be sent and summed in bfloat16 or wider, within the bound.
A program may use at most 64 MiB of HBM per device.

v0:
```python
import jax
import jax.numpy as jnp
from jax import lax
from jax.sharding import PartitionSpec as P

HEAD_DIM = 64
POOL_CH = 256
POOL_GROUPS = 4
WINDOW = 128
EPS = 1e-06
SHORT_REACHES = (8, 32)


def sent_together(arrays, axis, dim, along):
    ends, at = ([], 0)
    for a in arrays[:-1]:
        at += a.shape[along]
        ends.append(at)
    both = jnp.concatenate(arrays, axis=along)
    return tuple(jnp.split(lax.all_gather(both, axis, axis=dim, tiled=True), ends, axis=along))


def passed_along(block, axis, distance):
    devices = range(lax.axis_size(axis))
    route = [(i - distance, i) for i in devices if i - distance in devices]
    return lax.ppermute(block, axis, route)


def from_everyone(x, axis):
    copies = jnp.broadcast_to(x, (lax.axis_size(axis), *x.shape))
    return lax.all_to_all(copies, axis, split_axis=0, concat_axis=0, tiled=True)


def in_order(parts, dim):
    parts = jnp.moveaxis(parts, 0, dim)
    shape = parts.shape
    return parts.reshape(*shape[:dim], shape[dim] * shape[dim + 1], *shape[dim + 2 :])


def gathered_copies(x, axis, dim):
    parts = from_everyone(x, axis)
    return in_order(parts, dim)


def local(
    tokens_in,
    norm_gain,
    query_weight,
    key_weight,
    value_weight,
    pool_weight,
    sink_logit,
    pool_gain,
    attention_out_weight,
    pool_out_weight,
):
    widened = tokens_in.astype(jnp.float32)
    inverse = lax.rsqrt(jnp.mean(widened * widened, axis=1, keepdims=True) + EPS)
    normed = (widened * inverse * norm_gain).astype(jnp.bfloat16)
    all_rows = lax.all_gather(normed, "tp", axis=0, tiled=True)
    pieces = sent_together((query_weight, key_weight, value_weight, pool_weight), "sp", 0, 1)
    projected = tuple(
        (
            jnp.dot(all_rows, weight_piece, preferred_element_type=jnp.float32)
            for weight_piece in pieces
        )
    )
    query_rows, key_rows, value_rows, pool_rows = [
        projection.astype(jnp.bfloat16) for projection in projected
    ]
    seq_len = query_rows.shape[0]
    offset = lax.axis_index("sp") * seq_len
    halo_keys, halo_values, halo_pool = passed_along(
        (
            key_rows[seq_len - WINDOW :],
            value_rows[seq_len - WINDOW :],
            pool_rows[seq_len - WINDOW :],
        ),
        "sp",
        1,
    )
    kv_local = key_rows.shape[1] // HEAD_DIM
    heads_local = query_rows.shape[1] // HEAD_DIM
    group = heads_local // kv_local
    blocks = seq_len // WINDOW
    key_ext = jnp.concatenate([halo_keys, key_rows], axis=0).reshape(
        blocks + 1, WINDOW, kv_local, HEAD_DIM
    )
    value_ext = jnp.concatenate([halo_values, value_rows], axis=0).reshape(
        blocks + 1, WINDOW, kv_local, HEAD_DIM
    )
    key_pairs = jnp.concatenate([key_ext[:-1], key_ext[1:]], axis=1)
    value_pairs = jnp.concatenate([value_ext[:-1], value_ext[1:]], axis=1)
    query_blocks = query_rows.reshape(blocks, WINDOW, kv_local, group, HEAD_DIM)
    scores = jnp.einsum(
        "nqhgd,nkhd->nhgqk", query_blocks, key_pairs, preferred_element_type=jnp.float32
    ) * HEAD_DIM ** (-0.5)
    shape_mask = (blocks, WINDOW, 2 * WINDOW)
    q_index = lax.broadcasted_iota(jnp.int32, shape_mask, 1)
    k_index = lax.broadcasted_iota(jnp.int32, shape_mask, 2)
    block_index = lax.broadcasted_iota(jnp.int32, shape_mask, 0)
    distance = q_index + WINDOW - k_index
    key_position = offset + block_index * WINDOW + k_index - WINDOW
    allowed = (distance >= 0) & (distance < WINDOW) & (key_position >= 0)
    scores = jnp.where(allowed[:, None, None], scores, -jnp.inf)
    sinks = sink_logit.reshape(1, kv_local, group, 1, 1)
    peak = jnp.maximum(jnp.max(scores, axis=-1, keepdims=True), sinks)
    expo = jnp.exp(scores - peak)
    denom = jnp.sum(expo, axis=-1, keepdims=True) + jnp.exp(sinks - peak)
    probs = (expo / denom).astype(jnp.bfloat16)
    attended = jnp.einsum(
        "nhgqk,nkhd->nqhgd", probs, value_pairs, preferred_element_type=jnp.float32
    )
    attended = attended.astype(jnp.bfloat16).reshape(seq_len, heads_local * HEAD_DIM)
    pool_values = pool_rows.astype(jnp.float32)
    channels = pool_rows.shape[1]
    pool_ext = jnp.concatenate([halo_pool.astype(jnp.float32), pool_values], axis=0)
    running = jnp.concatenate(
        [jnp.zeros((1, channels), jnp.float32), jnp.cumsum(pool_ext, axis=0)], axis=0
    )
    group_id = lax.axis_index("tp") * channels // POOL_CH
    reach = jnp.where(
        group_id == 0, SHORT_REACHES[0], jnp.where(group_id == 1, SHORT_REACHES[1], WINDOW)
    ).astype(jnp.int32)
    upper = running[WINDOW + 1 :]
    lower = lax.dynamic_slice_in_dim(running, WINDOW + 1 - reach, seq_len, 0)
    position = offset + lax.broadcasted_iota(jnp.int32, (seq_len,), 0)
    counted = jnp.minimum(position + 1, reach).astype(jnp.float32)[:, None]
    windowed = (upper - lower) / counted
    own_sums = upper - running[WINDOW]
    device_total = own_sums[seq_len - 1]
    totals = gathered_copies(device_total[None, :], "sp", 0)
    earlier_rows = lax.broadcasted_iota(jnp.int32, (totals.shape[0], 1), 0) < lax.axis_index("sp")
    before = jnp.sum(jnp.where(earlier_rows, totals, 0.0), axis=0)
    cumulative = (before[None, :] + own_sums) / (position + 1).astype(jnp.float32)[:, None]
    pooled = jnp.where(group_id == POOL_GROUPS - 1, cumulative, windowed)
    pool_mixed = ((pooled - pool_values) * pool_gain).astype(jnp.bfloat16)
    out_attend, out_pool = sent_together((attention_out_weight, pool_out_weight), "sp", 1, 0)
    return lax.psum_scatter(
        (
            jnp.dot(attended, out_attend, preferred_element_type=jnp.float32)
            + jnp.dot(pool_mixed, out_pool, preferred_element_type=jnp.float32)
        ).astype(jnp.bfloat16),
        "tp",
        scatter_dimension=0,
        tiled=True,
    )


def solution(mesh):
    in_specs = (
        P(("sp", "tp"), None),
        P(),
        P("sp", "tp"),
        P("sp", "tp"),
        P("sp", "tp"),
        P("sp", "tp"),
        P("tp"),
        P("tp"),
        P("tp", "sp"),
        P("tp", "sp"),
    )
    out_specs = P(("sp", "tp"), None)
    return jax.shard_map(local, mesh=mesh, in_specs=in_specs, out_specs=out_specs, check_vma=False)
```

profile of v0, /device:TPU:0, one launch (start us, length us, event | category | flops | bytes accessed | tf_op | source)
XLA Modules:
  0.0 182.7 jit_solution(4462187103619193170)
XLA Ops:
  6.5 0.0 all-gather.6.cloned.1.call-start
  6.5 0.8 copy.33
  7.4 0.8 copy.34
  8.2 1.5 pad_maximum_fusion.3
  9.7 0.0 all-gather.6.cloned.1.call-update
  9.7 0.0 all-gather.4.cloned.1.call-start
  9.8 1.2 fusion.2
  11.0 1.9 %fusion.4 = bf16[96,2048]{1,0:T(8,128)(2,1)} fusion(bf16[96,2048]{1,0:T(8,128)(2,1)} %param.10, f32[2048]{0:T(1024)} %param.11, f32[96]{0:T(128)S(1)} %add_rsqrt_fusion), kind=kLoop, calls=%fused_computation.15 | loop fusion | flops 786432 | bytes 795008 | tf_op jit(solution)/shard_map/convert_element_type | solution.py:59
  12.9 0.0 all-gather.4.cloned.1.call-update
  12.9 0.0 all-gather.8.cloned.1.call-start
  13.0 0.0 copy-done.8
  13.0 0.0 copy-done.9
  13.0 0.6 pad_maximum_fusion.4
  13.6 0.0 all-gather.8.cloned.1.call-update
  13.8 1.0 fusion.8
  14.7 41.5 %all-gather.6.cloned.1.call-done = bf16[2048,384]{1,0:T(8,128)(2,1)} async-done(((bf16[128,384]{1,0:T(8,128)(2,1)}), bf16[2048,384]{1,0:T(8,128)(2,1)}) %all-gather.6.cloned.1.call-update) | async-done | bytes 1572880 | tf_op jit(solution)/shard_map/all_gather | solution.py:20
  56.2 28.7 %all-gather.4.cloned.1.call-done = bf16[768,2048]{1,0:T(8,128)(2,1)} async-done(((bf16[96,2048]{1,0:T(8,128)(2,1)}), bf16[768,2048]{1,0:T(8,128)(2,1)}) %all-gather.4.cloned.1.call-update) | async-done | bytes 3145744 | tf_op jit(solution)/shard_map/all_gather | solution.py:60
  84.9 3.2 %convolution_convert_fusion.3 = bf16[768,64]{0,1:T(8,128)(2,1)S(1)} fusion(bf16[768,2048]{1,0:T(8,128)(2,1)} %all-gather.4.cloned.1.call-done, bf16[2048,384]{1,0:T(8,128)(2,1)} %all-gather.6.cloned.1.call-done), kind=kOutput, calls=%fused_computation.9 | convolution fusion | flops 201375744 | bytes 3768320 | tf_op jit(solution)/shard_map/dot_general | solution.py:64
  88.1 0.6 slice.62
  88.7 0.0 copy-done.6
  88.8 0.1 slice.53
  88.9 0.0 copy-done
  88.9 2.2 %convolution_convert_fusion.4 = bf16[768,64]{0,1:T(8,128)(2,1)S(1)} fusion(bf16[768,2048]{1,0:T(8,128)(2,1)S(1)} %copy-done, bf16[2048,384]{1,0:T(8,128)(2,1)} %all-gather.6.cloned.1.call-done), kind=kOutput, calls=%fused_computation.10 | convolution fusion | flops 201375744 | bytes 3768320 | tf_op jit(solution)/shard_map/dot_general | solution.py:64
  91.1 0.6 slice.61
  91.8 0.1 slice.49
  91.9 4.0 %collective-permute-start.1 = (bf16[128,64]{0,1:T(8,128)(2,1)}, bf16[128,64]{0,1:T(8,128)(2,1)}, u32[]{:S(2)}, u32[]{:S(2)}) collective-permute-start(bf16[128,64]{0,1:T(8,128)(2,1)} %slice.62), channel_id=1, source_target_pairs={{0,8},{8,16},{16,24},{24,32},{32,40},{40,48},{48,56},{56,64},{64,7... | collective-permute-start | bytes 49160 | tf_op jit(solution)/shard_map/ppermute | solution.py:26
  95.9 0.6 copy.38
  96.5 3.4 %collective-permute-start = (bf16[128,64]{0,1:T(8,128)(2,1)}, bf16[128,64]{0,1:T(8,128)(2,1)}, u32[]{:S(2)}, u32[]{:S(2)}) collective-permute-start(bf16[128,64]{0,1:T(8,128)(2,1)} %slice.61), channel_id=1, source_target_pairs={{0,8},{8,16},{16,24},{24,32},{32,40},{40,48},{48,56},{56,64},{64,7... | collective-permute-start | bytes 49160 | tf_op jit(solution)/shard_map/ppermute | solution.py:26
  99.9 0.0 copy-done.4
  99.9 0.6 copy.36
  100.6 2.0 %fusion.45 = (f32[768,128]{1,0:T(8,128)S(1)}, bf16[768,128]{1,0:T(8,128)(2,1)S(1)}) fusion(bf16[768,2048]{1,0:T(8,128)(2,1)S(1)} %copy-done, bf16[2048,384]{1,0:T(8,128)(2,1)} %all-gather.6.cloned.1.call-done), kind=kOutput, calls=%fused_computation.79 | convolution fusion | flops 402849792 | bytes 4259840 | tf_op jit(solution)/shard_map/dot_general | solution.py:64
  102.6 0.7 copy-done.1
  103.2 0.6 slice.63
  103.8 3.1 %collective-permute-start.2 = (bf16[128,128]{1,0:T(8,128)(2,1)}, bf16[128,128]{1,0:T(8,128)(2,1)}, u32[]{:S(2)}, u32[]{:S(2)}) collective-permute-start(bf16[128,128]{1,0:T(8,128)(2,1)} %slice.63), channel_id=1, source_target_pairs={{0,8},{8,16},{16,24},{24,32},{32,40},{40,48},{48,56},{56,64},{64,7... | collective-permute-start | bytes 98312 | tf_op jit(solution)/shard_map/ppermute | solution.py:26
  106.9 2.7 %convolution_convert_fusion.1 = bf16[768,128]{1,0:T(8,128)(2,1)} fusion(bf16[768,2048]{1,0:T(8,128)(2,1)S(1)} %copy-done, bf16[2048,384]{1,0:T(8,128)(2,1)} %all-gather.6.cloned.1.call-done), kind=kOutput, calls=%fused_computation.6 | convolution fusion | flops 402751488 | bytes 3866624 | tf_op jit(solution)/shard_map/dot_general | solution.py:64
  109.6 1.1 reshape.121
  110.7 0.0 collective-permute-done.1
  110.8 0.9 pad_maximum_fusion.1
  111.7 0.0 copy-start.10
  111.7 0.1 slice.52
  111.8 1.5 fusion.44
  113.3 0.1 broadcast_maximum_fusion
  113.4 0.2 fusion
  113.7 0.1 exponential_add_fusion
  113.7 0.0 collective-permute-done
  113.8 0.7 pad_maximum_fusion.2
  114.5 0.1 slice.48
  114.7 0.4 fusion.1
  115.1 0.1 copy.42
  115.2 0.0 collective-permute-done.2
  115.2 0.8 convert_element_type.66
  116.0 0.3 fusion.17
  116.4 0.1 copy.44
  116.5 0.6 broadcast_in_dim.40
  117.1 6.1 %all-to-all-start = ((f32[16,1,128]{2,1,0:T(1,128)}), f32[16,1,128]{2,1,0:T(1,128)S(1)}, u32[]{:S(2)}, u32[]{:S(2)}) async-start(f32[16,1,128]{2,1,0:T(1,128)} %broadcast_in_dim.40), calls=%async_computation | async-start | bytes 16384 | tf_op jit(solution)/shard_map/all_to_all | solution.py:31
  123.3 0.0 reduce-scatter.2.cloned.1.call-start
  123.3 7.0 %all-gather.8.cloned.1.call-done = bf16[256,2048]{1,0:T(8,128)(2,1)} async-done(((bf16[256,128]{1,0:T(8,128)(2,1)}), bf16[256,2048]{1,0:T(8,128)(2,1)}) %all-gather.8.cloned.1.call-update) | async-done | bytes 1048592 | tf_op jit(solution)/shard_map/all_gather | solution.py:20
  130.3 4.8 %fusion.12 = f32[768,2048]{1,0:T(8,128)} fusion(bf16[256,2048]{1,0:T(8,128)(2,1)} %all-gather.8.cloned.1.call-done, bf16[16,8,6,128]{3,2,1,0:T(8,128)(2,1)S(1)} %bitcast.62), kind=kOutput, calls=%fused_computation.25 | convolution fusion | flops 402653184 | bytes 7012352 | tf_op jit(solution)/shard_map/dot_general | solution.py:141
  135.1 0.0 all-to-all-done
  135.1 0.1 select_reduce_fusion
  135.2 0.0 copy-done.2
  135.2 5.6 %add_convert_fusion = bf16[768,2048]{1,0:T(8,128)(2,1)} fusion(f32[768,2048]{1,0:T(8,128)} %fusion.12, bf16[256,2048]{1,0:T(8,128)(2,1)S(1)} %copy-done.3, s32[]{:T(128)S(6)} %select_n.38, f32[896,128]{1,0:T(8,128)S(1)} %bitcast.60, f32[768,128]{1,0:T(8,128)S(1)} %slice_subtract_fusion, f32[128]{0:T(128)S(1)} %copy-done.11, f32[768]{0:T(1024)S(1)} %get-tuple-element.9, ...), kind=kOutput, calls=%fused_computation | convolution fusion | flops 406683648 | bytes 11412485 | tf_op jit(solution)/shard_map/dot_general | solution.py:142
  140.8 0.0 reduce-scatter.2.cloned.1.call-update
  140.8 35.3 %reduce-scatter.2.cloned.1.call-done = bf16[96,2048]{1,0:T(8,128)(2,1)} async-done(((bf16[768,2048]{1,0:T(8,128)(2,1)}), bf16[96,2048]{1,0:T(8,128)(2,1)}) %reduce-scatter.2.cloned.1.call-update) | async-done | bytes 393232 | tf_op jit(solution)/shard_map/reduce_scatter | solution.py:139
  (30 shorter events, 0.2 us)
Async XLA Ops:
  6.5 6.4 %copy-start.8 = (bf16[128,128]{1,0:T(8,128)(2,1)S(1)}, bf16[128,128]{1,0:T(8,128)(2,1)}, u32[]{:S(2)}) copy-start(bf16[128,128]{1,0:T(8,128)(2,1)} %param.19) | copy-start | bytes 98308
  6.5 6.5 %copy-start.9 = (bf16[128,128]{1,0:T(8,128)(2,1)S(1)}, bf16[128,128]{1,0:T(8,128)(2,1)}, u32[]{:S(2)}) copy-start(bf16[128,128]{1,0:T(8,128)(2,1)} %param.18) | copy-start | bytes 98308
  6.5 49.7 %all-gather.6.cloned.1.call-start = ((), (), s32[]{:S(2)}) async-start(), calls=%async_computation.3 | async-start | bytes 1671168 | tf_op jit(solution)/shard_map/all_gather | solution.py:20
  9.7 75.1 %all-gather.4.cloned.1.call-start = ((), (), s32[]{:S(2)}) async-start(), calls=%async_computation.2 | async-start | bytes 3538944 | tf_op jit(solution)/shard_map/all_gather | solution.py:60
  12.9 117.4 %all-gather.8.cloned.1.call-start = ((), (), s32[]{:S(2)}) async-start(), calls=%async_computation.4 | async-start | bytes 1114112 | tf_op jit(solution)/shard_map/all_gather | solution.py:20
  84.9 4.0 %copy-start = (bf16[768,2048]{1,0:T(8,128)(2,1)S(1)}, bf16[768,2048]{1,0:T(8,128)(2,1)}, u32[]{:S(2)}) copy-start(bf16[768,2048]{1,0:T(8,128)(2,1)} %all-gather.4.cloned.1.call-done) | copy-start | bytes 9437188
  88.1 0.7 copy-start.6
  91.1 8.8 %copy-start.4 = (bf16[768,64]{0,1:T(8,128)(2,1)}, bf16[768,64]{0,1:T(8,128)(2,1)S(1)}, u32[]{:S(2)}) copy-start(bf16[768,64]{0,1:T(8,128)(2,1)S(1)} %convolution_convert_fusion.4) | copy-start | bytes 294916
  91.9 18.8 %collective-permute-start.1 = (bf16[128,64]{0,1:T(8,128)(2,1)}, bf16[128,64]{0,1:T(8,128)(2,1)}, u32[]{:S(2)}, u32[]{:S(2)}) collective-permute-start(bf16[128,64]{0,1:T(8,128)(2,1)} %slice.62), channel_id=1, source_target_pairs={{0,8},{8,16},{16,24},{24,32},{32,40},{40,48},{48,56},{56,64},{64,7... | collective-permute-start | bytes 49160 | tf_op jit(solution)/shard_map/ppermute | solution.py:26
  96.5 17.2 %collective-permute-start = (bf16[128,64]{0,1:T(8,128)(2,1)}, bf16[128,64]{0,1:T(8,128)(2,1)}, u32[]{:S(2)}, u32[]{:S(2)}) collective-permute-start(bf16[128,64]{0,1:T(8,128)(2,1)} %slice.61), channel_id=1, source_target_pairs={{0,8},{8,16},{16,24},{24,32},{32,40},{40,48},{48,56},{56,64},{64,7... | collective-permute-start | bytes 49160 | tf_op jit(solution)/shard_map/ppermute | solution.py:26
  102.6 0.7 copy-start.1
  103.8 11.4 %collective-permute-start.2 = (bf16[128,128]{1,0:T(8,128)(2,1)}, bf16[128,128]{1,0:T(8,128)(2,1)}, u32[]{:S(2)}, u32[]{:S(2)}) collective-permute-start(bf16[128,128]{1,0:T(8,128)(2,1)} %slice.63), channel_id=1, source_target_pairs={{0,8},{8,16},{16,24},{24,32},{32,40},{40,48},{48,56},{56,64},{64,7... | collective-permute-start | bytes 98312 | tf_op jit(solution)/shard_map/ppermute | solution.py:26
  111.7 1.7 copy-start.10
  111.8 1.9 %copy-start.5 = (bf16[768,64]{0,1:T(8,128)(2,1)S(1)}, bf16[768,64]{0,1:T(8,128)(2,1)}, u32[]{:S(2)}) copy-start(bf16[768,64]{0,1:T(8,128)(2,1)} %copy-done.4) | copy-start | bytes 294916
  113.3 1.3 copy-start.7
  117.1 18.0 %all-to-all-start = ((f32[16,1,128]{2,1,0:T(1,128)}), f32[16,1,128]{2,1,0:T(1,128)S(1)}, u32[]{:S(2)}, u32[]{:S(2)}) async-start(f32[16,1,128]{2,1,0:T(1,128)} %broadcast_in_dim.40), calls=%async_computation | async-start | bytes 16384 | tf_op jit(solution)/shard_map/all_to_all | solution.py:31
  123.3 52.8 %reduce-scatter.2.cloned.1.call-start = ((), (), s32[]{:S(2)}) async-start(), calls=%async_computation.5 | async-start | bytes 3538944 | tf_op jit(solution)/shard_map/reduce_scatter | solution.py:139
  130.3 4.9 %copy-start.2 = (bf16[768,128]{1,0:T(8,128)(2,1)S(1)}, bf16[768,128]{1,0:T(8,128)(2,1)}, u32[]{:S(2)}) copy-start(bf16[768,128]{1,0:T(8,128)(2,1)} %copy-done.1) | copy-start | bytes 589828
  130.3 4.9 %copy-start.3 = (bf16[256,2048]{1,0:T(8,128)(2,1)S(1)}, bf16[256,2048]{1,0:T(8,128)(2,1)}, u32[]{:S(2)}) copy-start(bf16[256,2048]{1,0:T(8,128)(2,1)} %all-gather.8.cloned.1.call-done) | copy-start | bytes 3145732
  130.3 4.9 %copy-start.11 = (f32[128]{0:T(128)S(1)}, f32[128]{0:T(128)}, u32[]{:S(2)}) copy-start(f32[128]{0:T(128)} %param.17) | copy-start | bytes 1540
Sparse Core Ops, SparseCore 0:
  9.9 46.2 all-gather.5
  57.9 26.9 all-gather.3
  87.0 43.2 all-gather.7
  141.0 35.1 reduce-scatter.1
where the time goes:
time: 183 us
  waiting for transfers between devices  112 us (61%)
  matrix products  22.4 us (12%)
  starting transfers between devices  16.7 us (9%)
  between operations  13.5 us (7%)
  other arithmetic  9.51 us (5%)
  local copies, waits for them, and re-layouts  8.08 us (4%)
    all_gather x2, waiting for transfers between devices, sent_together(): lax.all_gather(both, axis, axis=dim, tiled=True)  48.4 us
    reduce_scatter x1, waiting for transfers between devices, local(): lax.psum_scatter((jnp.dot(attended, out_attend, preferred_element_type=jn...  35.3 us
    all_gather x1, waiting for transfers between devices, local(): all_rows = lax.all_gather(normed, 'tp', axis=0, tiled=True)  28.7 us
    ppermute x3, starting transfers between devices, passed_along(): return lax.ppermute(block, axis, route)  10.4 us
    dot_general x4, matrix products, local(): jnp.dot(all_rows, weight_piece, preferred_element_type=jnp.float32)  10.1 us
    all_to_all x1, starting transfers between devices, from_everyone(): return lax.all_to_all(copies, axis, split_axis=0, concat_axis=0, tiled=True)  6.14 us
    dot_general x1, matrix products, local(): jnp.dot(pool_mixed, out_pool, preferred_element_type=jnp.float32)  5.6 us
    dot_general x1, matrix products, local(): jnp.dot(attended, out_attend, preferred_element_type=jnp.float32)  4.8 us
  transfers between devices with their start and end apart: 8, of which 4 were waited for; matrix products, arithmetic and copies ran while one was open for 17% of the time, Pallas kernels for 0%

commit v1 on v0

--- a/solution.py
+++ b/solution.py
@@ -57,7 +57,17 @@
     widened = tokens_in.astype(jnp.float32)
     inverse = lax.rsqrt(jnp.mean(widened * widened, axis=1, keepdims=True) + EPS)
     normed = (widened * inverse * norm_gain).astype(jnp.bfloat16)
-    all_rows = lax.all_gather(normed, "tp", axis=0, tiled=True)
+
+    def push_seats_all(payload):
+        return lax.all_to_all(
+            jnp.concatenate(tuple((payload for _ in range(lax.axis_size("tp")))), axis=0),
+            "tp",
+            0,
+            0,
+            tiled=True,
+        )
+
+    all_rows = push_seats_all(normed)
     pieces = sent_together((query_weight, key_weight, value_weight, pool_weight), "sp", 0, 1)
     projected = tuple(
         (

time: 183 us -> 154 us (0.84)
  waiting for transfers between devices: 112 us -> 74.4 us
  starting transfers between devices: 16.7 us -> 22.5 us
  other arithmetic: 9.51 us -> 11.9 us
    all_gather x2, waiting for transfers between devices: 48.4 us -> 2.3 us  [sent_together(): lax.all_gather(both, axis, axis=dim, tiled=True)]
    all_to_all x0 -> x1, waiting for transfers between devices: none -> 36.6 us  [push_seats_all(): lax.all_to_all(jnp.concatenate(tuple((payload for _ in range(lax.axis_siz...]
    all_gather x1 -> x0, waiting for transfers between devices: 28.7 us -> none  [local(): all_rows = lax.all_gather(normed, 'tp', axis=0, tiled=True)]
    all_to_all x0 -> x1, starting transfers between devices: none -> 4.71 us  [push_seats_all(): lax.all_to_all(jnp.concatenate(tuple((payload for _ in range(lax.axis_siz...]
    unnamed x0 -> x7, other arithmetic: none -> 4.18 us
    convert_element_type x1 -> x0, other arithmetic: 1.91 us -> none  [local(): normed = (widened * inverse * norm_gain).astype(jnp.bfloat16)]
    unnamed x26 -> x30, local copies, waits for them, and re-layouts: 2.4 us -> 4.04 us
  transfers between devices with their start and end apart: 8 -> 8, of which waited for: 4 -> 4; matrix products, arithmetic and copies ran while one was open for 17% -> 21% of each run, Pallas kernels for 0% -> 0%
where the time goes in v1:
time: 154 us; the launch traced here: 153 us
  waiting for transfers between devices  74.4 us (48%)
  starting transfers between devices  22.5 us (15%)
  matrix products  21.2 us (14%)
  between operations  13.5 us (9%)
  other arithmetic  11.9 us (8%)
  local copies, waits for them, and re-layouts  9.8 us (6%)
    all_to_all x1, waiting for transfers between devices, push_seats_all(): lax.all_to_all(jnp.concatenate(tuple((payload for _ in range(lax.axis_siz...  36.6 us
    reduce_scatter x1, waiting for transfers between devices, local(): lax.psum_scatter((jnp.dot(attended, out_attend, preferred_element_type=jn...  35.1 us
    ppermute x3, starting transfers between devices, passed_along(): return lax.ppermute(block, axis, route)  10.5 us
    dot_general x4, matrix products, local(): jnp.dot(all_rows, weight_piece, preferred_element_type=jnp.float32)  9.03 us
    all_to_all x1, starting transfers between devices, from_everyone(): return lax.all_to_all(copies, axis, split_axis=0, concat_axis=0, tiled=True)  7.21 us
    dot_general x1, matrix products, local(): jnp.dot(pool_mixed, out_pool, preferred_element_type=jnp.float32)  5.59 us
    dot_general x1, matrix products, local(): jnp.dot(attended, out_attend, preferred_element_type=jnp.float32)  4.8 us
    all_to_all x1, starting transfers between devices, push_seats_all(): lax.all_to_all(jnp.concatenate(tuple((payload for _ in range(lax.axis_siz...  4.71 us
  transfers between devices with their start and end apart: 8, of which 4 were waited for; matrix products, arithmetic and copies ran while one was open for 21% of the time, Pallas kernels for 0%

profile of v1, /device:TPU:0, one launch (start us, length us, event | category | flops | bytes accessed | tf_op | source)
XLA Modules:
  0.0 153.4 jit_solution(11612307629813194411)
XLA Ops:
  6.5 0.9 copy.33
  7.4 0.8 copy.34
  8.3 1.5 pad_maximum_fusion.3
  9.8 0.0 all-gather.3.cloned.1.call-update
  9.8 1.2 fusion.2
  11.0 1.2 constant_dynamic-update-slice_fusion.7
  12.2 1.2 constant_dynamic-update-slice_fusion.6
  13.3 1.2 constant_dynamic-update-slice_fusion.5
  14.5 0.2 constant_dynamic-update-slice_fusion.4
  14.7 0.2 constant_dynamic-update-slice_fusion.3
  14.9 0.2 constant_dynamic-update-slice_fusion.2
  15.0 0.2 constant_dynamic-update-slice_fusion.1
  15.2 0.2 constant_dynamic-update-slice_fusion
  15.4 0.0 copy-start.1
  15.4 1.6 %copy-done.1 = bf16[768,2048]{1,0:T(8,128)(2,1)} copy-done((bf16[768,2048]{1,0:T(8,128)(2,1)}, bf16[768,2048]{1,0:T(8,128)(2,1)S(1)}, u32[]{:S(2)}) %copy-start.1) | copy-done | bytes 3145752
  17.0 4.7 %all-to-all-start = ((bf16[8,96,2048]{2,1,0:T(8,128)(2,1)}), bf16[8,96,2048]{2,1,0:T(8,128)(2,1)S(1)}, u32[]{:S(2)}, u32[]{:S(2)}) async-start(bf16[8,96,2048]{2,1,0:T(8,128)(2,1)} %bitcast.64), calls=%async_computation | async-start | bytes 6291456 | tf_op jit(solution)/shard_map/all_to_all | solution.py:62
  21.7 0.0 all-gather.5.cloned.1.call-start
  21.8 0.6 pad_maximum_fusion.4
  22.4 0.0 all-gather.5.cloned.1.call-update
  22.5 1.0 fusion.8
  23.5 36.6 %all-to-all-done = bf16[8,96,2048]{2,1,0:T(8,128)(2,1)S(1)} async-done(((bf16[8,96,2048]{2,1,0:T(8,128)(2,1)}), bf16[8,96,2048]{2,1,0:T(8,128)(2,1)S(1)}, u32[]{:S(2)}, u32[]{:S(2)}) %all-to-all-start) | async-done | bytes 3145760 | tf_op jit(solution)/shard_map/all_to_all | solution.py:62
  60.1 2.1 %convolution_convert_fusion.3 = bf16[768,64]{0,1:T(8,128)(2,1)S(1)} fusion(bf16[768,2048]{1,0:T(8,128)(2,1)S(1)} %bitcast.60, bf16[2048,384]{1,0:T(8,128)(2,1)} %all-gather.3.cloned.1.call-done), kind=kOutput, calls=%fused_computation.9 | convolution fusion | flops 201375744 | bytes 3768320 | tf_op jit(solution)/shard_map/dot_general | solution.py:74
  62.3 0.7 slice.62
  62.9 0.0 copy-done.7
  62.9 0.1 slice.53
  63.0 2.2 %convolution_convert_fusion.4 = bf16[768,64]{0,1:T(8,128)(2,1)S(1)} fusion(bf16[768,2048]{1,0:T(8,128)(2,1)S(1)} %bitcast.61, bf16[2048,384]{1,0:T(8,128)(2,1)} %all-gather.3.cloned.1.call-done), kind=kOutput, calls=%fused_computation.10 | convolution fusion | flops 201375744 | bytes 3768320 | tf_op jit(solution)/shard_map/dot_general | solution.py:74
  65.3 0.6 slice.61
  65.9 0.1 slice.49
  66.0 4.0 %collective-permute-start.1 = (bf16[128,64]{0,1:T(8,128)(2,1)}, bf16[128,64]{0,1:T(8,128)(2,1)}, u32[]{:S(2)}, u32[]{:S(2)}) collective-permute-start(bf16[128,64]{0,1:T(8,128)(2,1)} %slice.62), channel_id=1, source_target_pairs={{0,8},{8,16},{16,24},{24,32},{32,40},{40,48},{48,56},{56,64},{64,7... | collective-permute-start | bytes 49160 | tf_op jit(solution)/shard_map/ppermute | solution.py:26
  70.0 0.7 copy.38
  70.7 3.4 %collective-permute-start = (bf16[128,64]{0,1:T(8,128)(2,1)}, bf16[128,64]{0,1:T(8,128)(2,1)}, u32[]{:S(2)}, u32[]{:S(2)}) collective-permute-start(bf16[128,64]{0,1:T(8,128)(2,1)} %slice.61), channel_id=1, source_target_pairs={{0,8},{8,16},{16,24},{24,32},{32,40},{40,48},{48,56},{56,64},{64,7... | collective-permute-start | bytes 49160 | tf_op jit(solution)/shard_map/ppermute | solution.py:26
  74.1 0.6 copy.36
  74.7 2.0 %fusion.45 = (f32[768,128]{1,0:T(8,128)S(1)}, bf16[768,128]{1,0:T(8,128)(2,1)S(1)}) fusion(bf16[768,2048]{1,0:T(8,128)(2,1)S(1)} %bitcast.62, bf16[2048,384]{1,0:T(8,128)(2,1)} %all-gather.3.cloned.1.call-done), kind=kOutput, calls=%fused_computation.87 | convolution fusion | flops 402849792 | bytes 4259840 | tf_op jit(solution)/shard_map/dot_general | solution.py:74
  76.8 0.7 copy-done.2
  77.4 0.6 slice.63
  78.0 3.1 %collective-permute-start.2 = (bf16[128,128]{1,0:T(8,128)(2,1)}, bf16[128,128]{1,0:T(8,128)(2,1)}, u32[]{:S(2)}, u32[]{:S(2)}) collective-permute-start(bf16[128,128]{1,0:T(8,128)(2,1)} %slice.63), channel_id=1, source_target_pairs={{0,8},{8,16},{16,24},{24,32},{32,40},{40,48},{48,56},{56,64},{64,7... | collective-permute-start | bytes 98312 | tf_op jit(solution)/shard_map/ppermute | solution.py:26
  81.2 2.7 %convolution_convert_fusion.1 = bf16[768,128]{1,0:T(8,128)(2,1)} fusion(bf16[768,2048]{1,0:T(8,128)(2,1)S(1)} %bitcast.63, bf16[2048,384]{1,0:T(8,128)(2,1)} %all-gather.3.cloned.1.call-done), kind=kOutput, calls=%fused_computation.6 | convolution fusion | flops 402751488 | bytes 3866624 | tf_op jit(solution)/shard_map/dot_general | solution.py:74
  83.9 1.1 reshape.123
  85.0 0.0 collective-permute-done.1
  85.0 0.9 pad_maximum_fusion.1
  85.9 0.1 slice.52
  86.1 1.4 fusion.44
  87.5 0.1 broadcast_maximum_fusion
  87.6 0.2 fusion
  87.9 0.1 exponential_add_fusion
  87.9 0.0 collective-permute-done
  88.0 0.7 pad_maximum_fusion.2
  88.7 0.1 slice.48
  88.9 0.4 fusion.1
  89.3 0.1 copy.42
  89.4 0.0 collective-permute-done.2
  89.4 0.8 convert_element_type.66
  90.2 0.3 fusion.17
  90.6 0.1 copy.44
  90.7 0.6 broadcast_in_dim.40
  91.3 7.2 %all-to-all-start.1 = ((f32[16,1,128]{2,1,0:T(1,128)}), f32[16,1,128]{2,1,0:T(1,128)S(1)}, u32[]{:S(2)}, u32[]{:S(2)}) async-start(f32[16,1,128]{2,1,0:T(1,128)} %broadcast_in_dim.40), calls=%async_computation.1 | async-start | bytes 16384 | tf_op jit(solution)/shard_map/all_to_all | solution.py:31
  98.6 0.0 reduce-scatter.2.cloned.1.call-start
  98.6 2.3 %all-gather.5.cloned.1.call-done = bf16[256,2048]{1,0:T(8,128)(2,1)} async-done(((bf16[256,128]{1,0:T(8,128)(2,1)}), bf16[256,2048]{1,0:T(8,128)(2,1)}) %all-gather.5.cloned.1.call-update) | async-done | bytes 1048592 | tf_op jit(solution)/shard_map/all_gather | solution.py:20
  100.9 4.8 %fusion.12 = f32[768,2048]{1,0:T(8,128)} fusion(bf16[256,2048]{1,0:T(8,128)(2,1)} %all-gather.5.cloned.1.call-done, bf16[16,8,6,128]{3,2,1,0:T(8,128)(2,1)S(1)} %bitcast.69), kind=kOutput, calls=%fused_computation.25 | convolution fusion | flops 402653184 | bytes 7012352 | tf_op jit(solution)/shard_map/dot_general | solution.py:151
  105.7 0.4 all-to-all-done.1
  106.1 0.1 select_reduce_fusion
  106.2 5.6 %add_convert_fusion = bf16[768,2048]{1,0:T(8,128)(2,1)} fusion(f32[768,2048]{1,0:T(8,128)} %fusion.12, bf16[256,2048]{1,0:T(8,128)(2,1)S(1)} %copy-done.4, s32[]{:T(128)S(6)} %select_n.38, f32[896,128]{1,0:T(8,128)S(1)} %bitcast.67, f32[768,128]{1,0:T(8,128)S(1)} %slice_subtract_fusion, f32[128]{0:T(128)S(1)} %copy-done.13, f32[768]{0:T(1024)S(1)} %get-tuple-element.9, ...), kind=kOutput, calls=%fused_computation | convolution fusion | flops 406683648 | bytes 11412485 | tf_op jit(solution)/shard_map/dot_general | solution.py:152
  111.8 0.0 reduce-scatter.2.cloned.1.call-update
  111.8 35.1 %reduce-scatter.2.cloned.1.call-done = bf16[96,2048]{1,0:T(8,128)(2,1)} async-done(((bf16[768,2048]{1,0:T(8,128)(2,1)}), bf16[96,2048]{1,0:T(8,128)(2,1)}) %reduce-scatter.2.cloned.1.call-update) | async-done | bytes 393232 | tf_op jit(solution)/shard_map/reduce_scatter | solution.py:149
  (40 shorter events, 0.2 us)
Async XLA Ops:
  6.5 8.0 %copy-start = (bf16[96,2048]{1,0:T(8,128)(2,1)S(1)}, bf16[96,2048]{1,0:T(8,128)(2,1)}, u32[]{:S(2)}) copy-start(bf16[96,2048]{1,0:T(8,128)(2,1)} %param.10) | copy-start | bytes 1179652
  6.5 8.0 %copy-start.8 = (f32[2048]{0:T(1024)S(1)}, f32[2048]{0:T(1024)}, u32[]{:S(2)}) copy-start(f32[2048]{0:T(1024)} %param.11) | copy-start | bytes 24580
  6.5 53.6 %all-gather.3.cloned.1.call-start = ((), (), s32[]{:S(2)}) async-start(), calls=%async_computation.3 | async-start | bytes 1671168 | tf_op jit(solution)/shard_map/all_gather | solution.py:20
  15.4 1.6 %copy-start.1 = (bf16[768,2048]{1,0:T(8,128)(2,1)}, bf16[768,2048]{1,0:T(8,128)(2,1)S(1)}, u32[]{:S(2)}) copy-start(bf16[768,2048]{1,0:T(8,128)(2,1)S(1)} %constant_dynamic-update-slice_fusion) | copy-start | bytes 9437188
  17.0 4.8 %copy-start.10 = (bf16[128,128]{1,0:T(8,128)(2,1)S(1)}, bf16[128,128]{1,0:T(8,128)(2,1)}, u32[]{:S(2)}) copy-start(bf16[128,128]{1,0:T(8,128)(2,1)} %param.19) | copy-start | bytes 98308
  17.0 4.8 %copy-start.11 = (bf16[128,128]{1,0:T(8,128)(2,1)S(1)}, bf16[128,128]{1,0:T(8,128)(2,1)}, u32[]{:S(2)}) copy-start(bf16[128,128]{1,0:T(8,128)(2,1)} %param.18) | copy-start | bytes 98308
  17.0 43.1 %all-to-all-start = ((bf16[8,96,2048]{2,1,0:T(8,128)(2,1)}), bf16[8,96,2048]{2,1,0:T(8,128)(2,1)S(1)}, u32[]{:S(2)}, u32[]{:S(2)}) async-start(bf16[8,96,2048]{2,1,0:T(8,128)(2,1)} %bitcast.64), calls=%async_computation | async-start | bytes 6291456 | tf_op jit(solution)/shard_map/all_to_all | solution.py:62
  21.7 79.2 %all-gather.5.cloned.1.call-start = ((), (), s32[]{:S(2)}) async-start(), calls=%async_computation.4 | async-start | bytes 1114112 | tf_op jit(solution)/shard_map/all_gather | solution.py:20
  62.2 0.7 copy-start.7
  65.3 8.8 %copy-start.5 = (bf16[768,64]{0,1:T(8,128)(2,1)}, bf16[768,64]{0,1:T(8,128)(2,1)S(1)}, u32[]{:S(2)}) copy-start(bf16[768,64]{0,1:T(8,128)(2,1)S(1)} %convolution_convert_fusion.4) | copy-start | bytes 294916
  66.0 19.0 %collective-permute-start.1 = (bf16[128,64]{0,1:T(8,128)(2,1)}, bf16[128,64]{0,1:T(8,128)(2,1)}, u32[]{:S(2)}, u32[]{:S(2)}) collective-permute-start(bf16[128,64]{0,1:T(8,128)(2,1)} %slice.62), channel_id=1, source_target_pairs={{0,8},{8,16},{16,24},{24,32},{32,40},{40,48},{48,56},{56,64},{64,7... | collective-permute-start | bytes 49160 | tf_op jit(solution)/shard_map/ppermute | solution.py:26
  70.7 17.3 %collective-permute-start = (bf16[128,64]{0,1:T(8,128)(2,1)}, bf16[128,64]{0,1:T(8,128)(2,1)}, u32[]{:S(2)}, u32[]{:S(2)}) collective-permute-start(bf16[128,64]{0,1:T(8,128)(2,1)} %slice.61), channel_id=1, source_target_pairs={{0,8},{8,16},{16,24},{24,32},{32,40},{40,48},{48,56},{56,64},{64,7... | collective-permute-start | bytes 49160 | tf_op jit(solution)/shard_map/ppermute | solution.py:26
  76.7 0.7 copy-start.2
  78.0 11.4 %collective-permute-start.2 = (bf16[128,128]{1,0:T(8,128)(2,1)}, bf16[128,128]{1,0:T(8,128)(2,1)}, u32[]{:S(2)}, u32[]{:S(2)}) collective-permute-start(bf16[128,128]{1,0:T(8,128)(2,1)} %slice.63), channel_id=1, source_target_pairs={{0,8},{8,16},{16,24},{24,32},{32,40},{40,48},{48,56},{56,64},{64,7... | collective-permute-start | bytes 98312 | tf_op jit(solution)/shard_map/ppermute | solution.py:26
  83.9 3.7 %copy-start.12 = (f32[2]{0:T(128)S(1)}, f32[2]{0:T(128)}, u32[]{:S(2)}) copy-start(f32[2]{0:T(128)} %param.16) | copy-start | bytes 28
  83.9 4.1 %copy-start.6 = (bf16[768,64]{0,1:T(8,128)(2,1)S(1)}, bf16[768,64]{0,1:T(8,128)(2,1)}, u32[]{:S(2)}) copy-start(bf16[768,64]{0,1:T(8,128)(2,1)} %copy-done.5) | copy-start | bytes 294916
  83.9 5.0 %copy-start.9 = (bf16[6,128,1,64]{1,3,0,2:T(8,128)(2,1)S(1)}, bf16[6,128,1,64]{1,3,0,2:T(8,128)(2,1)}, u32[]{:S(2)}) copy-start(bf16[6,128,1,64]{1,3,0,2:T(8,128)(2,1)} %copy.36) | copy-start | bytes 294916
  91.3 14.7 %all-to-all-start.1 = ((f32[16,1,128]{2,1,0:T(1,128)}), f32[16,1,128]{2,1,0:T(1,128)S(1)}, u32[]{:S(2)}, u32[]{:S(2)}) async-start(f32[16,1,128]{2,1,0:T(1,128)} %broadcast_in_dim.40), calls=%async_computation.1 | async-start | bytes 16384 | tf_op jit(solution)/shard_map/all_to_all | solution.py:31
  98.6 48.3 %reduce-scatter.2.cloned.1.call-start = ((), (), s32[]{:S(2)}) async-start(), calls=%async_computation.5 | async-start | bytes 3538944 | tf_op jit(solution)/shard_map/reduce_scatter | solution.py:149
  100.9 5.3 %copy-start.3 = (bf16[768,128]{1,0:T(8,128)(2,1)S(1)}, bf16[768,128]{1,0:T(8,128)(2,1)}, u32[]{:S(2)}) copy-start(bf16[768,128]{1,0:T(8,128)(2,1)} %copy-done.2) | copy-start | bytes 589828
  100.9 5.3 %copy-start.4 = (bf16[256,2048]{1,0:T(8,128)(2,1)S(1)}, bf16[256,2048]{1,0:T(8,128)(2,1)}, u32[]{:S(2)}) copy-start(bf16[256,2048]{1,0:T(8,128)(2,1)} %all-gather.5.cloned.1.call-done) | copy-start | bytes 3145732
  100.9 5.3 %copy-start.13 = (f32[128]{0:T(128)S(1)}, f32[128]{0:T(128)}, u32[]{:S(2)}) copy-start(f32[128]{0:T(128)} %param.17) | copy-start | bytes 1540
Sparse Core Ops, SparseCore 0:
  9.9 46.4 all-gather.2
  58.5 42.3 all-gather.4
  111.9 34.8 reduce-scatter.1
